TPU v7x, 512 devices: a whole 4x4x16 slice. The times are simulated.
512 devices in a mesh: fs: 16 (over y, x), tp: 32 (over z, core).
Axes of the slice: x: 4, y: 4, z: 16, core: 2. Of those that a mesh axis runs over, the one named last changes fastest.
Arguments:
- saved_input: bfloat16 [16384, 4096], P('fs', 'tp'), may hold values from -6 to 6
- query_cot: bfloat16 [16384, 4096], P('fs', 'tp'), may hold values from -6 to 6
- key_cot: bfloat16 [16384, 4096], P('fs', 'tp'), may hold values from -6 to 6
- query_master: float32 [4096, 4096], P('fs', 'tp'), may hold values from -0.09375 to 0.09375
- key_master: float32 [4096, 4096], P('fs', 'tp'), may hold values from -0.09375 to 0.09375
- query_basis: bfloat16 [4096, 256], P('fs'), may hold values from -3 to 3
- key_basis: bfloat16 [4096, 256], P('fs'), may hold values from -3 to 3
- query_first: float32 [256, 4096], P('fs', 'tp'), may hold values from -240 to 240
- query_second: float32 [256, 4096], P('fs', 'tp'), may hold values from 1000 to 20000
- key_first: float32 [256, 4096], P('fs', 'tp'), may hold values from -240 to 240
- key_second: float32 [256, 4096], P('fs', 'tp'), may hold values from 1000 to 20000
Outputs:
- query_step: float32 [4096, 4096], P('fs', 'tp')
- query_weight: float32 [4096, 4096], P('fs', 'tp')
- query_copy: bfloat16 [4096, 4096], P(None, 'tp')
- query_first_new: float32 [256, 4096], P('fs', 'tp')
- query_second_new: float32 [256, 4096], P('fs', 'tp')
- key_step: float32 [4096, 4096], P('fs', 'tp')
- key_weight: float32 [4096, 4096], P('fs', 'tp')
- key_copy: bfloat16 [4096, 4096], P(None, 'tp')
- key_first_new: float32 [256, 4096], P('fs', 'tp')
- key_second_new: float32 [256, 4096], P('fs', 'tp')
All inputs are finite; a program needn't handle non-finite values.
Results may differ from a plain program's by a relative error of at most 0.0065.
Values may be sent and summed in bfloat16 or wider, within the bound.
A program may use at most 64 MiB of HBM per device.

v0:
```python
import jax
import jax.numpy as jnp
from jax import lax
from jax.sharding import Mesh
from jax.sharding import PartitionSpec as P

D = 4096
HD = 128
FS = ("fs_0", "fs_1")
moment_decay = 0.8
square_decay = 0.9
square_floor = 1.0
norm_floor = 0.01
step_rate = 0.01


def in_one_piece(arrays, axis, dim, along):
    widths = [a.shape[along] for a in arrays]
    both = jnp.concatenate(arrays, axis=along)
    out = lax.all_gather(both, axis, axis=dim, tiled=True)
    return tuple(jnp.split(out, [sum(widths[:k]) for k in range(1, len(widths))], axis=along))


def cut_along(x, dim, count):
    lengths = x.shape
    pieces = x.reshape(*lengths[:dim], count, lengths[dim] // count, *lengths[dim + 1 :])
    return jnp.moveaxis(pieces, dim, 0)


def sent_and_summed(x, axis, dim):
    count = lax.axis_size(axis)
    pieces = lax.all_to_all(cut_along(x, dim, count), axis, 0, 0, tiled=True)
    return jnp.sum(pieces, axis=0)


def sent_to_all(x, axis):
    count = lax.axis_size(axis)
    return lax.all_to_all(jnp.broadcast_to(x[None], (count, *x.shape)), axis, 0, 0, tiled=True)


def in_order(pieces, dim):
    lengths = list(pieces.shape[1:])
    lengths[dim] *= pieces.shape[0]
    return jnp.moveaxis(pieces, 0, dim).reshape(lengths)


def gathered_copies(x, axis, dim):
    pieces = sent_to_all(x, axis)
    return in_order(pieces, dim)


def by_axis(x, axes):
    for axis in axes:
        x = lax.psum(x, axis)
    return x


def split_product(low_part, cot_part):
    upper = low_part.astype(jnp.bfloat16)
    lower = (low_part - upper.astype(jnp.float32)).astype(jnp.bfloat16)
    return jnp.dot(upper.T, cot_part, preferred_element_type=jnp.float32) + jnp.dot(
        lower.T, cot_part, preferred_element_type=jnp.float32
    )


def cot_rows(query_low, key_low, cot_wide, width):

    def low_rows(start, count):
        return jnp.concatenate(
            [
                split_product(query_low, cot_wide[:, :width]),
                split_product(key_low, cot_wide[:, width:]),
            ],
            axis=1,
        )

    return low_rows


def head_squares(update):
    by_head = update.reshape(update.shape[0], -1, HD)
    return jnp.sum(by_head * by_head, axis=(0, 2))


def apply_scale(update, total):
    scale = 1.0 / jnp.sqrt(total / (D * HD) + norm_floor)
    by_head = update.reshape(update.shape[0], -1, HD)
    return (by_head * scale[None, :, None]).reshape(update.shape)


def body(
    saved_input,
    query_cot,
    key_cot,
    query_master,
    key_master,
    query_basis,
    key_basis,
    query_first,
    query_second,
    key_first,
    key_second,
):
    width = query_cot.shape[1]
    low_count = query_first.shape[0]
    cotangents = jnp.concatenate([query_cot, key_cot], axis=1)
    inputs = lax.all_gather(saved_input, "tp", axis=1, tiled=True)
    bases = in_one_piece((query_basis, key_basis), FS, 0, 1)
    query_low = jnp.dot(inputs, bases[0], preferred_element_type=jnp.float32)
    key_low = jnp.dot(inputs, bases[1], preferred_element_type=jnp.float32)
    low_rows = cot_rows(query_low, key_low, cotangents, width)
    projected = sent_and_summed(low_rows(jnp.int32(0), low_count * lax.axis_size(FS)), FS, 0)
    firsts = jnp.concatenate([query_first, key_first], axis=1)
    seconds = jnp.concatenate([query_second, key_second], axis=1)
    first_new = moment_decay * firsts + (1.0 - moment_decay) * projected
    second_new = square_decay * seconds + (1.0 - square_decay) * projected * projected
    ratio = (first_new / jnp.sqrt(second_new + square_floor)).astype(jnp.bfloat16)
    piece = gathered_copies(ratio, FS, 0)
    query_update = jnp.dot(query_basis, piece[:, :width], preferred_element_type=jnp.float32)
    key_update = jnp.dot(key_basis, piece[:, width:], preferred_element_type=jnp.float32)
    query_total, key_total = (
        by_axis(head_squares(query_update), FS),
        by_axis(head_squares(key_update), FS),
    )
    query_step = apply_scale(query_update, query_total)
    key_step = apply_scale(key_update, key_total)
    query_weight = query_master - step_rate * query_step
    key_weight = key_master - step_rate * key_step
    copies = in_one_piece(
        (query_weight.astype(jnp.bfloat16), key_weight.astype(jnp.bfloat16)), FS, 0, 1
    )
    return (
        query_step,
        query_weight,
        copies[0],
        first_new[:, :width],
        second_new[:, :width],
        key_step,
        key_weight,
        copies[1],
        first_new[:, width:],
        second_new[:, width:],
    )


def solution(mesh):
    torus = Mesh(mesh.devices.reshape(4, 4, mesh.shape["tp"]), ("fs_0", "fs_1", "tp"))
    in_specs = (
        P(FS, "tp"),
        P(FS, "tp"),
        P(FS, "tp"),
        P(FS, "tp"),
        P(FS, "tp"),
        P(FS, None),
        P(FS, None),
        P(FS, "tp"),
        P(FS, "tp"),
        P(FS, "tp"),
        P(FS, "tp"),
    )
    out_specs = (
        P(FS, "tp"),
        P(FS, "tp"),
        P(None, "tp"),
        P(FS, "tp"),
        P(FS, "tp"),
        P(FS, "tp"),
        P(FS, "tp"),
        P(None, "tp"),
        P(FS, "tp"),
        P(FS, "tp"),
    )
    return jax.shard_map(body, mesh=torus, in_specs=in_specs, out_specs=out_specs, check_vma=False)
```

profile of v0, /device:TPU:2, one launch (start us, length us, event | category | flops | bytes accessed | tf_op | source)
XLA Modules:
  0.0 306.8 jit_solution(4869370095504522026)
XLA Ops:
  7.2 0.0 copy-start
  7.2 0.0 all-gather.4.cloned.1.call-start
  7.2 1.7 pad_maximum_fusion
  9.0 0.0 all-gather.4.cloned.1.call-update
  9.0 0.0 all-gather.6.cloned.1.call-start
  9.0 0.7 all-gather.6.cloned.1.call-update
  9.7 73.1 %all-gather.4.cloned.1.call-done = bf16[4096,512]{1,0:T(8,128)(2,1)} async-done(((bf16[256,512]{1,0:T(8,128)(2,1)}), bf16[4096,512]{1,0:T(8,128)(2,1)}) %all-gather.4.cloned.1.call-update) | async-done | bytes 4194320 | tf_op jit(solution)/shard_map/all_gather | solution.py:20
  82.8 97.5 %all-gather.6.cloned.1.call-done = bf16[1024,4096]{1,0:T(8,128)(2,1)} async-done(((bf16[1024,128]{1,0:T(8,128)(2,1)}), bf16[1024,4096]{1,0:T(8,128)(2,1)}) %all-gather.6.cloned.1.call-update) | async-done | bytes 8388624 | tf_op jit(solution)/shard_map/all_gather | solution.py:107
  180.2 0.0 copy-start.10
  180.2 0.0 copy-start.11
  180.2 6.5 %fusion.4 = f32[1024,256]{0,1:T(8,128)S(1)} fusion(bf16[1024,4096]{1,0:T(8,128)(2,1)} %all-gather.6.cloned.1.call-done, bf16[4096,512]{1,0:T(8,128)(2,1)} %all-gather.4.cloned.1.call-done), kind=kOutput, calls=%fused_computation.4 | convolution fusion | flops 2147483648 | bytes 11534336 | tf_op jit(solution)/shard_map/dot_general | solution.py:109
  186.8 0.0 copy-done
  186.8 0.3 fusion.14
  187.1 0.3 convolution_add_fusion.1
  187.5 0.0 copy-done.10
  187.5 0.4 copy-done.11
  187.8 0.0 copy-start.1
  187.8 2.4 fusion.7
  190.2 0.0 copy-done.1
  190.2 0.0 copy-start.6
  190.2 0.0 copy-start.7
  190.3 0.0 copy-start.8
  190.3 0.0 copy-start.9
  190.3 0.0 copy-start.4
  190.3 0.0 copy-start.5
  190.3 0.0 copy-start.2
  190.3 0.0 copy-start.3
  190.3 0.3 fusion.11
  190.7 0.3 convolution_add_fusion
  191.0 0.1 copy.29
  191.1 14.8 %all_to_all.10 = f32[16,16,256]{2,1,0:T(8,128)S(1)} all-to-all(f32[16,16,256]{2,1,0:T(8,128)S(1)} %bitcast.24), channel_id=1, replica_groups=mesh['fs_0'=4,'fs_1'=4,'tp'=32] {'fs_0','fs_1'}, dimensions={0} | all-to-all | bytes 524288 | tf_op jit(solution)/shard_map/all_to_all | solution.py:32
  206.0 0.0 copy-done.6
  206.0 0.0 copy-done.7
  206.0 0.0 copy-done.8
  206.0 0.0 copy-done.9
  206.0 0.7 broadcast_in_dim.2
  206.7 4.8 %all-to-all-start.1 = ((bf16[16,16,256]{2,1,0:T(8,128)(2,1)}), bf16[16,16,256]{2,1,0:T(8,128)(2,1)S(1)}, u32[]{:S(2)}, u32[]{:S(2)}) async-start(bf16[16,16,256]{2,1,0:T(8,128)(2,1)} %broadcast_in_dim.2), calls=%async_computation.1 | async-start | bytes 262144 | tf_op jit(solution)/shard_map/all_to_all | solution.py:38
  211.5 0.0 all-gather.8.cloned.1.call-start
  211.5 0.0 copy-done.4
  211.5 0.1 copy.30
  211.6 0.0 copy-done.5
  211.6 0.1 copy.31
  211.7 6.4 %all-to-all-done.1 = bf16[16,16,256]{2,1,0:T(8,128)(2,1)S(1)} async-done(((bf16[16,16,256]{2,1,0:T(8,128)(2,1)}), bf16[16,16,256]{2,1,0:T(8,128)(2,1)S(1)}, u32[]{:S(2)}, u32[]{:S(2)}) %all-to-all-start.1) | async-done | bytes 131104 | tf_op jit(solution)/shard_map/all_to_all | solution.py:38
  218.2 0.0 copy-done.2
  218.2 0.8 multiply_reduce_fusion.1
  219.0 0.0 copy-done.3
  219.0 0.8 multiply_reduce_fusion
  219.8 9.2 %all-reduce.1 = (f32[1]{0:T(128)}, f32[1]{0:T(128)}) all-reduce(f32[1]{0:T(128)} %bitcast.4, f32[1]{0:T(128)} %bitcast.7), channel_id=1, replica_groups=mesh['fs_0'=4,'fs_1'=4,'tp'=32] {'fs_0'}, use_global_device_ids=true, to_apply=%region_2.0 | all-reduce | flops 2 | bytes 16 | tf_op jit(solution)/shard_map/psum | solution.py:54
  229.0 9.8 %all-reduce = (f32[1]{0:T(128)}, f32[1]{0:T(128)}) all-reduce(f32[1]{0:T(128)} %get-tuple-element.32, f32[1]{0:T(128)} %get-tuple-element.33), channel_id=1, replica_groups=mesh['fs_0'=4,'fs_1'=4,'tp'=32] {'fs_1'}, use_global_device_ids=true, to_apply=%region_3.0 | all-reduce | flops 2 | bytes 16 | tf_op jit(solution)/shard_map/psum | solution.py:54
  240.2 0.1 fusion.22
  240.2 0.7 pad_maximum_fusion.2
  240.9 0.0 all-gather.8.cloned.1.call-update
  240.9 0.6 fusion.27
  241.5 0.8 copy.32
  242.3 0.8 copy.33
  243.1 0.8 copy.35
  243.8 0.8 copy.36
  244.6 51.4 %all-gather.8.cloned.1.call-done = bf16[4096,256]{0,1:T(8,128)(2,1)} async-done(((bf16[256,256]{0,1:T(8,128)(2,1)}), bf16[4096,256]{0,1:T(8,128)(2,1)}) %all-gather.8.cloned.1.call-update) | async-done | bytes 2097168 | tf_op jit(solution)/shard_map/all_gather | solution.py:20
  296.0 1.7 fusion.26
  297.6 1.3 copy.34
  299.0 1.3 copy.37
  (3 shorter events, 0.1 us)
Async XLA Ops:
  7.2 179.6 %copy-start = (bf16[1024,128]{1,0:T(8,128)(2,1)S(1)}, bf16[1024,128]{1,0:T(8,128)(2,1)}, u32[]{:S(2)}) copy-start(bf16[1024,128]{1,0:T(8,128)(2,1)} %param.12) | copy-start | bytes 786436
  7.2 75.6 %all-gather.4.cloned.1.call-start = ((), (), s32[]{:S(2)}) async-start(), calls=%async_computation.2 | async-start | bytes 4456448 | tf_op jit(solution)/shard_map/all_gather | solution.py:20
  9.0 171.3 %all-gather.6.cloned.1.call-start = ((), (), s32[]{:S(2)}) async-start(), calls=%async_computation.3 | async-start | bytes 8650752 | tf_op jit(solution)/shard_map/all_gather | solution.py:107
  180.2 7.2 %copy-start.10 = (bf16[1024,4096]{1,0:T(8,128)(2,1)S(1)}, bf16[1024,4096]{1,0:T(8,128)(2,1)}, u32[]{:S(2)}) copy-start(bf16[1024,4096]{1,0:T(8,128)(2,1)} %all-gather.6.cloned.1.call-done) | copy-start | bytes 25165828
  180.2 7.6 %copy-start.11 = (bf16[4096,512]{1,0:T(8,128)(2,1)S(1)}, bf16[4096,512]{1,0:T(8,128)(2,1)}, u32[]{:S(2)}) copy-start(bf16[4096,512]{1,0:T(8,128)(2,1)} %all-gather.4.cloned.1.call-done) | copy-start | bytes 12582916
  187.8 2.4 copy-start.1
  190.2 15.7 %copy-start.6 = (f32[16,128]{1,0:T(8,128)S(1)}, f32[16,128]{1,0:T(8,128)}, u32[]{:S(2)}) copy-start(f32[16,128]{1,0:T(8,128)} %param.21) | copy-start | bytes 24580
  190.2 15.7 %copy-start.7 = (f32[16,128]{1,0:T(8,128)S(1)}, f32[16,128]{1,0:T(8,128)}, u32[]{:S(2)}) copy-start(f32[16,128]{1,0:T(8,128)} %param.19) | copy-start | bytes 24580
  190.3 15.7 %copy-start.8 = (f32[16,128]{1,0:T(8,128)S(1)}, f32[16,128]{1,0:T(8,128)}, u32[]{:S(2)}) copy-start(f32[16,128]{1,0:T(8,128)} %param.20) | copy-start | bytes 24580
  190.3 15.7 %copy-start.9 = (f32[16,128]{1,0:T(8,128)S(1)}, f32[16,128]{1,0:T(8,128)}, u32[]{:S(2)}) copy-start(f32[16,128]{1,0:T(8,128)} %param.18) | copy-start | bytes 24580
  190.3 21.2 %copy-start.4 = (f32[256,128]{1,0:T(8,128)S(1)}, f32[256,128]{1,0:T(8,128)}, u32[]{:S(2)}) copy-start(f32[256,128]{1,0:T(8,128)} %param.14) | copy-start | bytes 393220
  190.3 21.3 %copy-start.5 = (f32[256,128]{1,0:T(8,128)S(1)}, f32[256,128]{1,0:T(8,128)}, u32[]{:S(2)}) copy-start(f32[256,128]{1,0:T(8,128)} %param.15) | copy-start | bytes 393220
  190.3 27.9 %copy-start.2 = (bf16[256,256]{1,0:T(8,128)(2,1)S(1)}, bf16[256,256]{1,0:T(8,128)(2,1)}, u32[]{:S(2)}) copy-start(bf16[256,256]{1,0:T(8,128)(2,1)} %param.16) | copy-start | bytes 393220
  190.3 28.7 %copy-start.3 = (bf16[256,256]{1,0:T(8,128)(2,1)S(1)}, bf16[256,256]{1,0:T(8,128)(2,1)}, u32[]{:S(2)}) copy-start(bf16[256,256]{1,0:T(8,128)(2,1)} %param.17) | copy-start | bytes 393220
  206.7 11.5 %all-to-all-start.1 = ((bf16[16,16,256]{2,1,0:T(8,128)(2,1)}), bf16[16,16,256]{2,1,0:T(8,128)(2,1)S(1)}, u32[]{:S(2)}, u32[]{:S(2)}) async-start(bf16[16,16,256]{2,1,0:T(8,128)(2,1)} %broadcast_in_dim.2), calls=%async_computation.1 | async-start | bytes 262144 | tf_op jit(solution)/shard_map/all_to_all | solution.py:38
  211.5 84.5 %all-gather.8.cloned.1.call-start = ((), (), s32[]{:S(2)}) async-start(), calls=%async_computation.4 | async-start | bytes 2228224 | tf_op jit(solution)/shard_map/all_gather | solution.py:20
Sparse Core Ops, SparseCore 0:
  11.6 71.1 all-gather.3
  84.8 95.3 all-gather.5
  241.1 54.8 all-gather.7
where the time goes:
time: 307 us
  waiting for transfers between devices  229 us (75%)
  blocking collectives  33.8 us (11%)
  between operations  15.4 us (5%)
  matrix products  11.8 us (4%)
  local copies, waits for them, and re-layouts  9.34 us (3%)
  starting transfers between devices  4.88 us (2%)
    all_gather x2, waiting for transfers between devices, in_one_piece(): out = lax.all_gather(both, axis, axis=dim, tiled=True)  124 us
    all_gather x1, waiting for transfers between devices, body(): inputs = lax.all_gather(saved_input, 'tp', axis=1, tiled=True)  97.5 us
    psum x2, blocking collectives, by_axis(): x = lax.psum(x, axis)  19 us
    all_to_all x1, blocking collectives, sent_and_summed(): pieces = lax.all_to_all(cut_along(x, dim, count), axis, 0, 0, tiled=True)  14.8 us
    dot_general x1, matrix products, body(): query_low = jnp.dot(inputs, bases[0], preferred_element_type=jnp.float32)  6.54 us
    all_to_all x1, waiting for transfers between devices, sent_to_all(): lax.all_to_all(jnp.broadcast_to(x[None], (count, *x.shape)), axis, 0, 0,...  6.45 us
    unnamed x32, local copies, waits for them, and re-layouts  6.25 us
  transfers between devices with their start and end apart: 4, of which 4 were waited for; matrix products, arithmetic and copies ran while one was open for 1% of the time, Pallas kernels for 0%

commit v1 on v0

--- a/solution.py
+++ b/solution.py
@@ -3,6 +3,7 @@
 from jax import lax
 from jax.sharding import Mesh
 from jax.sharding import PartitionSpec as P
+from jax.lax import all_to_all, axis_size
 
 D = 4096
 HD = 128
@@ -104,7 +105,8 @@
     width = query_cot.shape[1]
     low_count = query_first.shape[0]
     cotangents = jnp.concatenate([query_cot, key_cot], axis=1)
-    inputs = lax.all_gather(saved_input, "tp", axis=1, tiled=True)
+    base_arr = all_to_all(jnp.stack([saved_input for _ in range(axis_size("tp"))], 0), "tp", 0, 0)
+    inputs = jnp.concatenate(base_arr, 1)
     bases = in_one_piece((query_basis, key_basis), FS, 0, 1)
     query_low = jnp.dot(inputs, bases[0], preferred_element_type=jnp.float32)
     key_low = jnp.dot(inputs, bases[1], preferred_element_type=jnp.float32)

time: 307 us -> 524 us (1.71)
  waiting for transfers between devices: 229 us -> 423 us
  starting transfers between devices: 4.88 us -> 20.6 us
    all_to_all x0 -> x1, waiting for transfers between devices: none -> 289 us  [body(): all_to_all(jnp.stack([saved_input for _ in range(axis_size('tp'))], 0), '...]
    all_gather x1 -> x0, waiting for transfers between devices: 97.5 us -> none  [body(): inputs = lax.all_gather(saved_input, 'tp', axis=1, tiled=True)]
    all_to_all x0 -> x1, starting transfers between devices: none -> 15.7 us  [body(): all_to_all(jnp.stack([saved_input for _ in range(axis_size('tp'))], 0), '...]
where the time goes in v1:
time: 524 us
  waiting for transfers between devices  423 us (81%)
  blocking collectives  33.8 us (6%)
  starting transfers between devices  20.6 us (4%)
  between operations  15.7 us (3%)
  matrix products  15.2 us (3%)
  local copies, waits for them, and re-layouts  14.4 us (3%)
    all_to_all x1, waiting for transfers between devices, body(): all_to_all(jnp.stack([saved_input for _ in range(axis_size('tp'))], 0), '...  289 us
    all_gather x2, waiting for transfers between devices, in_one_piece(): out = lax.all_gather(both, axis, axis=dim, tiled=True)  128 us
    psum x2, blocking collectives, by_axis(): x = lax.psum(x, axis)  19 us
    all_to_all x1, starting transfers between devices, body(): all_to_all(jnp.stack([saved_input for _ in range(axis_size('tp'))], 0), '...  15.7 us
    all_to_all x1, blocking collectives, sent_and_summed(): pieces = lax.all_to_all(cut_along(x, dim, count), axis, 0, 0, tiled=True)  14.8 us
  transfers between devices with their start and end apart: 4, of which 4 were waited for; matrix products, arithmetic and copies ran while one was open for 1% of the time, Pallas kernels for 0%

profile of v1, /device:TPU:2, one launch (start us, length us, event | category | flops | bytes accessed | tf_op | source)
XLA Modules:
  0.0 523.9 jit_solution(643318494548698429)
XLA Ops:
  7.2 0.0 copy-start
  7.2 1.1 copy.29
  8.3 4.3 stack.2
  12.6 0.0 copy-start.3
  12.6 0.0 copy-start.4
  12.6 15.7 %all-to-all-start = ((bf16[32,1024,128]{1,2,0:T(8,128)(2,1)}), bf16[32,1024,128]{1,2,0:T(8,128)(2,1)}, u32[]{:S(2)}, u32[]{:S(2)}) async-start(bf16[32,1024,128]{1,2,0:T(8,128)(2,1)} %stack.2), calls=%async_computation | async-start | bytes 16777216 | tf_op jit(solution)/shard_map/all_to_all | solution.py:108
  28.4 0.0 all-gather.3.cloned.1.call-start
  28.4 0.0 copy-done.3
  28.5 0.0 copy-done.4
  28.5 0.7 pad_maximum_fusion
  29.2 0.0 all-gather.3.cloned.1.call-update
  29.2 71.3 %all-gather.3.cloned.1.call-done = bf16[4096,512]{1,0:T(8,128)(2,1)} async-done(((bf16[256,512]{1,0:T(8,128)(2,1)}), bf16[4096,512]{1,0:T(8,128)(2,1)}) %all-gather.3.cloned.1.call-update) | async-done | bytes 4194320 | tf_op jit(solution)/shard_map/all_gather | solution.py:21
  100.5 288.6 %all-to-all-done = bf16[32,1024,128]{1,2,0:T(8,128)(2,1)} async-done(((bf16[32,1024,128]{1,2,0:T(8,128)(2,1)}), bf16[32,1024,128]{1,2,0:T(8,128)(2,1)}, u32[]{:S(2)}, u32[]{:S(2)}) %all-to-all-start) | async-done | bytes 8388640 | tf_op jit(solution)/shard_map/all_to_all | solution.py:108
  389.1 0.0 copy-start.1
  389.1 6.5 %fusion.4 = f32[1024,256]{0,1:T(8,128)S(1)} fusion(bf16[1024,4096]{0,1:T(8,128)(2,1)} %bitcast.1, bf16[4096,512]{1,0:T(8,128)(2,1)} %all-gather.3.cloned.1.call-done), kind=kOutput, calls=%fused_computation.4 | convolution fusion | flops 2147483648 | bytes 11534336 | tf_op jit(solution)/shard_map/dot_general | solution.py:111
  395.7 0.0 copy-done
  395.7 0.3 fusion.14
  396.0 0.3 convolution_add_fusion.1
  396.3 0.0 copy-done.1
  396.4 0.0 copy-start.2
  396.4 5.8 %fusion.7 = f32[1024,256]{0,1:T(8,128)S(1)} fusion(bf16[1024,4096]{0,1:T(8,128)(2,1)} %bitcast.1, bf16[4096,512]{1,0:T(8,128)(2,1)S(1)} %copy-done.1), kind=kOutput, calls=%fused_computation.5 | convolution fusion | flops 2147483648 | bytes 11534336 | tf_op jit(solution)/shard_map/dot_general | solution.py:112
  402.2 0.0 copy-done.2
  402.2 0.0 copy-start.7
  402.2 0.0 copy-start.8
  402.2 0.0 copy-start.9
  402.2 0.0 copy-start.10
  402.2 0.0 copy-start.5
  402.2 0.0 copy-start.6
  402.2 0.3 fusion.11
  402.6 0.3 convolution_add_fusion
  402.9 0.1 copy.30
  403.1 14.8 %all_to_all.15 = f32[16,16,256]{2,1,0:T(8,128)S(1)} all-to-all(f32[16,16,256]{2,1,0:T(8,128)S(1)} %bitcast.27), channel_id=1, replica_groups=mesh['fs_0'=4,'fs_1'=4,'tp'=32] {'fs_0','fs_1'}, dimensions={0} | all-to-all | bytes 524288 | tf_op jit(solution)/shard_map/all_to_all | solution.py:33
  417.9 0.0 copy-done.7
  417.9 0.0 copy-done.8
  417.9 0.0 copy-done.9
  417.9 0.0 copy-done.10
  417.9 0.7 broadcast_in_dim.2
  418.6 4.8 all-to-all-start.2
  423.4 0.0 all-gather.5.cloned.1.call-start
  423.4 0.0 copy-done.5
  423.4 0.1 copy.31
  423.5 0.0 copy-done.6
  423.5 0.1 copy.32
  423.6 6.4 %all-to-all-done.2 = bf16[16,16,256]{2,1,0:T(8,128)(2,1)S(1)} async-done(((bf16[16,16,256]{2,1,0:T(8,128)(2,1)}), bf16[16,16,256]{2,1,0:T(8,128)(2,1)S(1)}, u32[]{:S(2)}, u32[]{:S(2)}) %all-to-all-start.2) | async-done | bytes 131104 | tf_op jit(solution)/shard_map/all_to_all | solution.py:39
  430.1 0.8 multiply_reduce_fusion
  430.9 0.8 multiply_reduce_fusion.1
  431.7 9.2 %all-reduce.1 = (f32[1]{0:T(128)}, f32[1]{0:T(128)}) all-reduce(f32[1]{0:T(128)} %bitcast.7, f32[1]{0:T(128)} %bitcast.10), channel_id=1, replica_groups=mesh['fs_0'=4,'fs_1'=4,'tp'=32] {'fs_0'}, use_global_device_ids=true, to_apply=%region_2.0 | all-reduce | flops 2 | bytes 16 | tf_op jit(solution)/shard_map/psum | solution.py:55
  440.9 9.8 %all-reduce = (f32[1]{0:T(128)}, f32[1]{0:T(128)}) all-reduce(f32[1]{0:T(128)} %get-tuple-element.32, f32[1]{0:T(128)} %get-tuple-element.33), channel_id=1, replica_groups=mesh['fs_0'=4,'fs_1'=4,'tp'=32] {'fs_1'}, use_global_device_ids=true, to_apply=%region_3.0 | all-reduce | flops 2 | bytes 16 | tf_op jit(solution)/shard_map/psum | solution.py:55
  452.1 0.1 fusion.22
  452.1 0.7 pad_maximum_fusion.2
  452.8 0.0 all-gather.5.cloned.1.call-update
  452.8 0.6 fusion.27
  453.5 0.8 copy.33
  454.2 0.8 copy.34
  455.0 0.8 copy.36
  455.7 0.8 copy.37
  456.5 56.3 %all-gather.5.cloned.1.call-done = bf16[4096,256]{0,1:T(8,128)(2,1)} async-done(((bf16[256,256]{0,1:T(8,128)(2,1)}), bf16[4096,256]{0,1:T(8,128)(2,1)}) %all-gather.5.cloned.1.call-update) | async-done | bytes 2097168 | tf_op jit(solution)/shard_map/all_gather | solution.py:21
  512.8 1.7 fusion.26
  514.5 1.3 copy.35
  515.8 1.3 copy.38
  (3 shorter events, 0.1 us)
Async XLA Ops:
  7.2 388.5 %copy-start = (bf16[1024,128]{1,0:T(8,128)(2,1)S(1)}, bf16[1024,128]{1,0:T(8,128)(2,1)}, u32[]{:S(2)}) copy-start(bf16[1024,128]{1,0:T(8,128)(2,1)} %param.12) | copy-start | bytes 786436
  12.6 15.8 %copy-start.3 = (bf16[256,256]{1,0:T(8,128)(2,1)S(1)}, bf16[256,256]{1,0:T(8,128)(2,1)}, u32[]{:S(2)}) copy-start(bf16[256,256]{1,0:T(8,128)(2,1)} %param.17) | copy-start | bytes 393220
  12.6 15.8 %copy-start.4 = (bf16[256,256]{1,0:T(8,128)(2,1)S(1)}, bf16[256,256]{1,0:T(8,128)(2,1)}, u32[]{:S(2)}) copy-start(bf16[256,256]{1,0:T(8,128)(2,1)} %param.16) | copy-start | bytes 393220
  12.6 376.5 %all-to-all-start = ((bf16[32,1024,128]{1,2,0:T(8,128)(2,1)}), bf16[32,1024,128]{1,2,0:T(8,128)(2,1)}, u32[]{:S(2)}, u32[]{:S(2)}) async-start(bf16[32,1024,128]{1,2,0:T(8,128)(2,1)} %stack.2), calls=%async_computation | async-start | bytes 16777216 | tf_op jit(solution)/shard_map/all_to_all | solution.py:108
  28.4 72.1 %all-gather.3.cloned.1.call-start = ((), (), s32[]{:S(2)}) async-start(), calls=%async_computation.3 | async-start | bytes 4456448 | tf_op jit(solution)/shard_map/all_gather | solution.py:21
  389.1 7.2 %copy-start.1 = (bf16[4096,512]{1,0:T(8,128)(2,1)S(1)}, bf16[4096,512]{1,0:T(8,128)(2,1)}, u32[]{:S(2)}) copy-start(bf16[4096,512]{1,0:T(8,128)(2,1)} %all-gather.3.cloned.1.call-done) | copy-start | bytes 12582916
  396.4 5.8 %copy-start.2 = (bf16[1024,128]{1,0:T(8,128)(2,1)S(1)}, bf16[1024,128]{1,0:T(8,128)(2,1)}, u32[]{:S(2)}) copy-start(bf16[1024,128]{1,0:T(8,128)(2,1)} %param.13) | copy-start | bytes 786436
  402.2 15.7 %copy-start.7 = (f32[16,128]{1,0:T(8,128)S(1)}, f32[16,128]{1,0:T(8,128)}, u32[]{:S(2)}) copy-start(f32[16,128]{1,0:T(8,128)} %param.21) | copy-start | bytes 24580
  402.2 15.7 %copy-start.8 = (f32[16,128]{1,0:T(8,128)S(1)}, f32[16,128]{1,0:T(8,128)}, u32[]{:S(2)}) copy-start(f32[16,128]{1,0:T(8,128)} %param.19) | copy-start | bytes 24580
  402.2 15.7 %copy-start.9 = (f32[16,128]{1,0:T(8,128)S(1)}, f32[16,128]{1,0:T(8,128)}, u32[]{:S(2)}) copy-start(f32[16,128]{1,0:T(8,128)} %param.20) | copy-start | bytes 24580
  402.2 15.7 %copy-start.10 = (f32[16,128]{1,0:T(8,128)S(1)}, f32[16,128]{1,0:T(8,128)}, u32[]{:S(2)}) copy-start(f32[16,128]{1,0:T(8,128)} %param.18) | copy-start | bytes 24580
  402.2 21.2 %copy-start.5 = (f32[256,128]{1,0:T(8,128)S(1)}, f32[256,128]{1,0:T(8,128)}, u32[]{:S(2)}) copy-start(f32[256,128]{1,0:T(8,128)} %param.14) | copy-start | bytes 393220
  402.2 21.3 %copy-start.6 = (f32[256,128]{1,0:T(8,128)S(1)}, f32[256,128]{1,0:T(8,128)}, u32[]{:S(2)}) copy-start(f32[256,128]{1,0:T(8,128)} %param.15) | copy-start | bytes 393220
  418.6 11.5 %all-to-all-start.2 = ((bf16[16,16,256]{2,1,0:T(8,128)(2,1)}), bf16[16,16,256]{2,1,0:T(8,128)(2,1)S(1)}, u32[]{:S(2)}, u32[]{:S(2)}) async-start(bf16[16,16,256]{2,1,0:T(8,128)(2,1)} %broadcast_in_dim.2), calls=%async_computation.2 | async-start | bytes 262144 | tf_op jit(solution)/shard_map/all_to_all | solution.py:39
  423.4 89.4 %all-gather.5.cloned.1.call-start = ((), (), s32[]{:S(2)}) async-start(), calls=%async_computation.4 | async-start | bytes 2228224 | tf_op jit(solution)/shard_map/all_gather | solution.py:21
Sparse Core Ops, SparseCore 0:
  32.8 67.6 all-gather.2
  453.0 59.7 all-gather.4
